TPU v7x, 512 devices: a 8x2x16 block of a 8x8x16 slice. The times are simulated.
512 devices in a mesh: grp: 2 (over y), sp: 32 (over z, core), tp: 8 (over x).
Axes of the slice: x: 8, y: 2, z: 16, core: 2. Of those that a mesh axis runs over, the one named last changes fastest.
The devices are a block of a 8x8x16 slice.
Arguments:
- tokens: bfloat16 [32768, 2048], P(('grp', 'sp'), 'tp'), parts along dimension 0, may hold values from -140 to 140, as said below
- mix_gain: bfloat16 [2, 2048], replicated, may hold values from 0.099609375 to 1.8984375
- gate_weight: bfloat16 [2, 2048, 2048], P(None, 'sp', 'tp'), may hold values from -0.125 to 0.125
- mix_weight: bfloat16 [2, 2048, 2048], P(None, 'sp', 'tp'), may hold values from -0.125 to 0.125
- value_weight: bfloat16 [2, 2048, 2048], P(None, 'sp', 'tp'), may hold values from -0.125 to 0.125
- out_weight: bfloat16 [2, 2048, 2048], P(None, 'sp', 'tp'), may hold values from -0.125 to 0.125
- conv_taps: bfloat16 [2, 3, 2048], P(None, None, 'tp'), may hold values from -3.5 to 3.5
Outputs:
- result_stream: bfloat16 [32768, 2048], P(('grp', 'sp'), 'tp'), parts along dimension 0
There are 2 independent parts, one for each index of `grp`. A program takes and returns all parts, laid end to end along the dimension named above; an argument that names none is the same for every part. Nothing has to cross between parts.
Inputs may be any that keep to these rules, and one draw needn't show every extreme that they name: `tokens`: activations with feature scales of several sizes.
All inputs are finite; a program needn't handle non-finite values.
Results may differ from a plain program's by a relative error of at most 0.015.
Values may be sent and summed in bfloat16 or wider, within the bound.
No kernel may reach another device: no remote copies, remote signals or barrier semaphores. Data moves between devices by JAX's collectives and lax.ppermute only.
A program may use at most 64 MiB of HBM per device.

v0:
```python
import jax
import jax.numpy as jnp
from jax import lax
from jax.sharding import PartitionSpec as P

EPS = 1e-06


def passed_along(x, axis, by):
    devices = lax.axis_size(axis)
    pairs = [(i, i + by) for i in range(devices) if 0 <= i + by < devices]
    return lax.ppermute(x, axis, pairs)


def in_one_piece(arrays, axis, dim, along):
    ends, at = ([], 0)
    for a in arrays[:-1]:
        at += a.shape[along]
        ends.append(at)
    both = jnp.concatenate(arrays, axis=along)
    return tuple(jnp.split(lax.all_gather(both, axis, axis=dim, tiled=True), ends, axis=along))


def in_order(pieces, dim):
    dims = list(pieces.shape[1:])
    dims[dim] *= pieces.shape[0]
    return jnp.moveaxis(pieces, 0, dim).reshape(dims)


def copy_for_each(x, axis):
    copies = jnp.broadcast_to(x, (lax.axis_size(axis), *x.shape))
    return lax.all_to_all(copies, axis, split_axis=0, concat_axis=0, tiled=True)


def collect(x, axis, dim):
    return in_order(copy_for_each(x, axis), dim)


def normed_rows(rows, gain):
    wide_rows = rows.astype(jnp.float32)
    factor = lax.rsqrt(jnp.mean(wide_rows * wide_rows, axis=1, keepdims=True) + EPS)
    return (wide_rows * factor * gain.astype(jnp.float32)).astype(jnp.bfloat16)


def convolve(carried, before, tap_rows):
    padded = jnp.concatenate([before, carried], axis=0)
    row_count = carried.shape[0]
    result = jnp.zeros_like(carried)
    for tap_index in range(tap_rows.shape[0]):
        result = (
            result
            + tap_rows[tap_index].astype(jnp.float32) * padded[tap_index : tap_index + row_count]
        )
    return result


def shards(tokens, mix_gain, gate_weight, mix_weight, value_weight, out_weight, conv_taps):
    layer_count = gate_weight.shape[0]
    conv_reach = conv_taps.shape[1] - 1
    fringe_depth = conv_reach * layer_count
    before_rows = passed_along(tokens[tokens.shape[0] - fringe_depth :], "sp", 1)
    stream = jnp.concatenate([before_rows, tokens], axis=0)
    gathered = in_one_piece((gate_weight, mix_weight, value_weight, out_weight), "sp", 1, 0)
    channels = gate_weight.shape[2]
    for layer_index in range(layer_count):
        whole = collect(stream, "tp", 1)
        normed = normed_rows(whole, mix_gain[layer_index])
        gate = jnp.dot(normed, gathered[0][layer_index], preferred_element_type=jnp.float32)
        inner = jnp.dot(normed, gathered[1][layer_index], preferred_element_type=jnp.float32)
        values = jnp.dot(normed, gathered[2][layer_index], preferred_element_type=jnp.float32)
        gate = gate.astype(jnp.bfloat16)
        inner = inner.astype(jnp.bfloat16)
        values = values.astype(jnp.bfloat16)
        carried = inner.astype(jnp.float32) * values.astype(jnp.float32)
        before = jnp.zeros((conv_reach, channels), jnp.float32)
        conv = convolve(carried, before, conv_taps[layer_index])
        mixed = (gate.astype(jnp.float32) * conv).astype(jnp.bfloat16)
        mixed_all = lax.all_gather(mixed, "tp", axis=1, tiled=True)
        product = jnp.dot(mixed_all, gathered[3][layer_index], preferred_element_type=jnp.float32)
        stream = (stream.astype(jnp.float32) + product).astype(jnp.bfloat16)
    return stream[fringe_depth:]


def solution(mesh):
    return jax.shard_map(
        shards,
        mesh=mesh,
        in_specs=(
            P(("grp", "sp"), "tp"),
            P(),
            P(None, "sp", "tp"),
            P(None, "sp", "tp"),
            P(None, "sp", "tp"),
            P(None, "sp", "tp"),
            P(None, None, "tp"),
        ),
        out_specs=P(("grp", "sp"), "tp"),
        check_vma=False,
    )
```

profile of v0, /device:TPU:66, one launch (start us, length us, event | category | flops | bytes accessed | tf_op | source)
XLA Modules:
  0.0 306.0 jit_solution(15098368979078359198)
XLA Ops:
  6.6 1.7 pad_maximum_fusion.1
  8.3 0.7 slice.88
  9.0 1.8 collective-permute-start
  10.8 0.8 collective-permute-done
  11.6 1.0 pad_maximum_fusion
  12.6 1.5 broadcast_in_dim.4
  14.1 43.5 %all-to-all-start = ((bf16[8,516,256]{2,1,0:T(8,128)(2,1)}), bf16[8,516,256]{2,1,0:T(8,128)(2,1)S(1)}, u32[]{:S(2)}, u32[]{:S(2)}) async-start(bf16[8,516,256]{2,1,0:T(8,128)(2,1)} %broadcast_in_dim.4), calls=%async_computation | async-start | bytes 4259840 | tf_op jit(solution)/shard_map/all_to_all | solution.py:32
  57.8 51.2 %all-to-all-done = bf16[8,516,256]{2,1,0:T(8,128)(2,1)S(1)} async-done(((bf16[8,516,256]{2,1,0:T(8,128)(2,1)}), bf16[8,516,256]{2,1,0:T(8,128)(2,1)S(1)}, u32[]{:S(2)}, u32[]{:S(2)}) %all-to-all-start) | async-done | bytes 2113568 | tf_op jit(solution)/shard_map/all_to_all | solution.py:32
  109.0 0.5 fusion
  109.5 0.6 fusion.7
  110.0 0.4 copy.8
  110.5 0.1 pad.8
  110.6 0.7 copy.10
  111.3 12.6 %all-gather.4.cloned.1.call-done = bf16[8,2048,256]{2,1,0:T(8,128)(2,1)} async-done(((bf16[8,64,256]{2,1,0:T(8,128)(2,1)}), bf16[8,2048,256]{2,1,0:T(8,128)(2,1)}) %all-gather.4.cloned.1.call-update) | async-done | bytes 8388624 | tf_op jit(solution)/shard_map/all_gather | solution.py:21
  123.9 2.0 fusion.13
  125.9 2.0 fusion.12
  128.0 2.7 fusion.10
  130.8 49.9 %all-gather.6.cloned.1.call-done = bf16[516,2048]{1,0:T(8,128)(2,1)} async-done(((bf16[516,256]{1,0:T(8,128)(2,1)}), bf16[516,2048]{1,0:T(8,128)(2,1)}) %all-gather.6.cloned.1.call-update) | async-done | bytes 2113552 | tf_op jit(solution)/shard_map/all_gather | solution.py:78
  180.7 2.6 add_convert_fusion
  183.3 1.5 broadcast_in_dim.5
  184.8 5.6 %all-to-all-start.1 = ((bf16[8,516,256]{2,1,0:T(8,128)(2,1)}), bf16[8,516,256]{2,1,0:T(8,128)(2,1)S(1)}, u32[]{:S(2)}, u32[]{:S(2)}) async-start(bf16[8,516,256]{2,1,0:T(8,128)(2,1)} %broadcast_in_dim.5), calls=%async_computation.1 | async-start | bytes 4259840 | tf_op jit(solution)/shard_map/all_to_all | solution.py:32
  190.3 45.0 %all-to-all-done.1 = bf16[8,516,256]{2,1,0:T(8,128)(2,1)S(1)} async-done(((bf16[8,516,256]{2,1,0:T(8,128)(2,1)}), bf16[8,516,256]{2,1,0:T(8,128)(2,1)S(1)}, u32[]{:S(2)}, u32[]{:S(2)}) %all-to-all-start.1) | async-done | bytes 2113568 | tf_op jit(solution)/shard_map/all_to_all | solution.py:32
  235.3 0.5 fusion.3
  235.9 0.6 fusion.6
  236.4 0.4 copy.9
  237.0 0.7 copy.11
  237.7 2.0 fusion.19
  239.7 2.0 fusion.18
  241.7 2.7 fusion.16
  244.5 51.6 %all-gather.8.cloned.1.call-done = bf16[516,2048]{1,0:T(8,128)(2,1)} async-done(((bf16[516,256]{1,0:T(8,128)(2,1)}), bf16[516,2048]{1,0:T(8,128)(2,1)}) %all-gather.8.cloned.1.call-update) | async-done | bytes 2113552 | tf_op jit(solution)/shard_map/all_gather | solution.py:78
  296.0 2.6 fusion.20
  298.6 0.8 fusion.22
  (19 shorter events, 0.4 us)
Async XLA Ops:
  6.5 117.4 %all-gather.4.cloned.1.call-start = ((), (), s32[]{:S(2)}) async-start(), calls=%async_computation.2 | async-start | bytes 8650752 | tf_op jit(solution)/shard_map/all_gather | solution.py:21
  9.0 2.6 collective-permute-start
  14.1 43.5 %copy-start.1 = (bf16[2,2048]{1,0:T(2,128)(2,1)S(1)}, bf16[2,2048]{1,0:T(2,128)(2,1)}, u32[]{:S(2)}) copy-start(bf16[2,2048]{1,0:T(2,128)(2,1)} %param.8) | copy-start | bytes 24580
  14.1 43.6 %copy-start.2 = (bf16[2,3,256]{2,0,1:T(2,128)(2,1)S(1)}, bf16[2,3,256]{2,0,1:T(2,128)(2,1)}, u32[]{:S(2)}) copy-start(bf16[2,3,256]{2,0,1:T(2,128)(2,1)} %param.13) | copy-start | bytes 9220
  14.1 94.8 %all-to-all-start = ((bf16[8,516,256]{2,1,0:T(8,128)(2,1)}), bf16[8,516,256]{2,1,0:T(8,128)(2,1)S(1)}, u32[]{:S(2)}, u32[]{:S(2)}) async-start(bf16[8,516,256]{2,1,0:T(8,128)(2,1)} %broadcast_in_dim.4), calls=%async_computation | async-start | bytes 4259840 | tf_op jit(solution)/shard_map/all_to_all | solution.py:32
  57.7 123.0 %all-gather.6.cloned.1.call-start = ((), (), s32[]{:S(2)}) async-start(), calls=%async_computation.3 | async-start | bytes 2396160 | tf_op jit(solution)/shard_map/all_gather | solution.py:78
  127.9 52.7 %copy-start = (bf16[512,256]{1,0:T(8,128)(2,1)S(1)}, bf16[512,256]{1,0:T(8,128)(2,1)}, u32[]{:S(2)}) copy-start(bf16[512,256]{1,0:T(8,128)(2,1)} %param.7) | copy-start | bytes 786436
  184.8 50.6 %all-to-all-start.1 = ((bf16[8,516,256]{2,1,0:T(8,128)(2,1)}), bf16[8,516,256]{2,1,0:T(8,128)(2,1)S(1)}, u32[]{:S(2)}, u32[]{:S(2)}) async-start(bf16[8,516,256]{2,1,0:T(8,128)(2,1)} %broadcast_in_dim.5), calls=%async_computation.1 | async-start | bytes 4259840 | tf_op jit(solution)/shard_map/all_to_all | solution.py:32
  190.3 105.7 %all-gather.8.cloned.1.call-start = ((), (), s32[]{:S(2)}) async-start(), calls=%async_computation.4 | async-start | bytes 2396160 | tf_op jit(solution)/shard_map/all_gather | solution.py:78
Sparse Core Ops, SparseCore 0:
  9.5 114.3 all-gather.3
  130.9 49.7 all-gather.5
  244.6 51.3 all-gather.7
where the time goes:
time: 307 us; the launch traced here: 306 us
  waiting for transfers between devices  211 us (69%)
  starting transfers between devices  50.9 us (17%)
  matrix products  18.6 us (6%)
  between operations  13.3 us (4%)
  local copies, waits for them, and re-layouts  6.28 us (2%)
  other arithmetic  5.67 us (2%)
    all_gather x2, waiting for transfers between devices, shards(): mixed_all = lax.all_gather(mixed, 'tp', axis=1, tiled=True)  101 us
    all_to_all x2, waiting for transfers between devices, copy_for_each(): return lax.all_to_all(copies, axis, split_axis=0, concat_axis=0, tiled=True)  96.2 us
    all_to_all x2, starting transfers between devices, copy_for_each(): return lax.all_to_all(copies, axis, split_axis=0, concat_axis=0, tiled=True)  49.1 us
    all_gather x1, waiting for transfers between devices, in_one_piece(): lax.all_gather(both, axis, axis=dim, tiled=True)  12.6 us
  transfers between devices with their start and end apart: 6, of which 6 were waited for; matrix products, arithmetic and copies ran while one was open for 2% of the time, Pallas kernels for 0%

commit v1 on v0

--- a/solution.py
+++ b/solution.py
@@ -75,7 +75,16 @@
         before = jnp.zeros((conv_reach, channels), jnp.float32)
         conv = convolve(carried, before, conv_taps[layer_index])
         mixed = (gate.astype(jnp.float32) * conv).astype(jnp.bfloat16)
-        mixed_all = lax.all_gather(mixed, "tp", axis=1, tiled=True)
+        ways = lax.axis_size("tp")
+        up = [(d, (d + 1) % ways) for d in range(ways)]
+        down = [(d, (d - 1) % ways) for d in range(ways)]
+        earlier, later = ([mixed], [mixed])
+        for _ in range(ways // 2):
+            earlier.append(lax.ppermute(earlier[-1], "tp", up))
+        for _ in range((ways - 1) // 2):
+            later.append(lax.ppermute(later[-1], "tp", down))
+        line = jnp.concatenate([*earlier[::-1], *later[1:]], axis=1)
+        mixed_all = jnp.roll(line, (lax.axis_index("tp") - ways // 2) * mixed.shape[1], axis=1)
         product = jnp.dot(mixed_all, gathered[3][layer_index], preferred_element_type=jnp.float32)
         stream = (stream.astype(jnp.float32) + product).astype(jnp.bfloat16)
     return stream[fringe_depth:]

time: 307 us -> 292 us (0.951)
  the two profiles are of different devices: /device:TPU:66 before, /device:TPU:78 now
where the time goes in v1:
time: 292 us; the launch traced here: 291 us
  waiting for transfers between devices  147 us (50%)
  starting transfers between devices  104 us (36%)
  between operations  13.9 us (5%)
  matrix products  12 us (4%)
  local copies, waits for them, and re-layouts  8.54 us (3%)
  other arithmetic  5.66 us (2%)
    all_to_all x2, waiting for transfers between devices, copy_for_each(): return lax.all_to_all(copies, axis, split_axis=0, concat_axis=0, tiled=True)  89.5 us
    all_to_all x2, starting transfers between devices, copy_for_each(): return lax.all_to_all(copies, axis, split_axis=0, concat_axis=0, tiled=True)  49.8 us
    ppermute x8, starting transfers between devices, shards(): earlier.append(lax.ppermute(earlier[-1], 'tp', up))  40.6 us
    ppermute x8, waiting for transfers between devices, shards(): earlier.append(lax.ppermute(earlier[-1], 'tp', up))  26.9 us
    all_gather x1, waiting for transfers between devices, in_one_piece(): lax.all_gather(both, axis, axis=dim, tiled=True)  17.2 us
    ppermute x6, waiting for transfers between devices, shards(): later.append(lax.ppermute(later[-1], 'tp', down))  12.3 us
    ppermute x6, starting transfers between devices, shards(): later.append(lax.ppermute(later[-1], 'tp', down))  12.2 us
  transfers between devices with their start and end apart: 18, of which 16 were waited for; matrix products, arithmetic and copies ran while one was open for 2% of the time, Pallas kernels for 0%

profile of v1, /device:TPU:78, one launch (start us, length us, event | category | flops | bytes accessed | tf_op | source)
XLA Modules:
  0.0 291.3 jit_solution(17690352403935190446)
XLA Ops:
  9.0 1.8 collective-permute-start
  14.2 42.7 %all-to-all-start = ((bf16[8,516,256]{2,1,0:T(8,128)(2,1)}), bf16[8,516,256]{2,1,0:T(8,128)(2,1)S(1)}, u32[]{:S(2)}, u32[]{:S(2)}) async-start(bf16[8,516,256]{2,1,0:T(8,128)(2,1)} %broadcast_in_dim.4), calls=%async_computation | async-start | bytes 4259840 | tf_op jit(solution)/shard_map/all_to_all | solution.py:32
  56.9 46.6 %all-to-all-done = bf16[8,516,256]{2,1,0:T(8,128)(2,1)S(1)} async-done(((bf16[8,516,256]{2,1,0:T(8,128)(2,1)}), bf16[8,516,256]{2,1,0:T(8,128)(2,1)S(1)}, u32[]{:S(2)}, u32[]{:S(2)}) %all-to-all-start) | async-done | bytes 2113568 | tf_op jit(solution)/shard_map/all_to_all | solution.py:32
  105.9 17.2 %all-gather.2.cloned.1.call-done = bf16[8,2048,256]{2,1,0:T(8,128)(2,1)} async-done(((bf16[8,64,256]{2,1,0:T(8,128)(2,1)}), bf16[8,2048,256]{2,1,0:T(8,128)(2,1)}) %all-gather.2.cloned.1.call-update) | async-done | bytes 8388624 | tf_op jit(solution)/shard_map/all_gather | solution.py:21
  123.1 2.0 fusion.22
  125.1 2.0 fusion.21
  127.2 2.0 fusion.19
  129.2 2.4 collective-permute-start.1
  131.5 8.1 %collective-permute-done.1 = bf16[516,256]{1,0:T(8,128)(2,1)S(1)} collective-permute-done((bf16[516,256]{1,0:T(8,128)(2,1)S(1)}, bf16[516,256]{1,0:T(8,128)(2,1)S(1)}, u32[]{:S(2)}, u32[]{:S(2)}) %collective-permute-start.1) | collective-permute-done | bytes 264224 | tf_op jit(solution)/shard_map/ppermute | solution.py:83
  139.6 3.6 %collective-permute-start.2 = (bf16[516,256]{1,0:T(8,128)(2,1)S(1)}, bf16[516,256]{1,0:T(8,128)(2,1)S(1)}, u32[]{:S(2)}, u32[]{:S(2)}) collective-permute-start(bf16[516,256]{1,0:T(8,128)(2,1)S(1)} %collective-permute-done.1), channel_id=1, source_target_pairs={{0,1},{1,2},{2,3},{3,4},{4,5},{5,6},{6,7},{7,0},{8,9},{9,10},{10,1... | collective-permute-start | bytes 792584 | tf_op jit(solution)/shard_map/ppermute | solution.py:83
  143.2 2.3 collective-permute-start.5
  145.5 3.7 %collective-permute-done.2 = bf16[516,256]{1,0:T(8,128)(2,1)S(1)} collective-permute-done((bf16[516,256]{1,0:T(8,128)(2,1)S(1)}, bf16[516,256]{1,0:T(8,128)(2,1)S(1)}, u32[]{:S(2)}, u32[]{:S(2)}) %collective-permute-start.2) | collective-permute-done | bytes 264224 | tf_op jit(solution)/shard_map/ppermute | solution.py:83
  149.2 4.8 %collective-permute-start.3 = (bf16[516,256]{1,0:T(8,128)(2,1)S(1)}, bf16[516,256]{1,0:T(8,128)(2,1)S(1)}, u32[]{:S(2)}, u32[]{:S(2)}) collective-permute-start(bf16[516,256]{1,0:T(8,128)(2,1)S(1)} %collective-permute-done.2), channel_id=1, source_target_pairs={{0,1},{1,2},{2,3},{3,4},{4,5},{5,6},{6,7},{7,0},{8,9},{9,10},{10,1... | collective-permute-start | bytes 792584 | tf_op jit(solution)/shard_map/ppermute | solution.py:83
  154.0 2.0 collective-permute-start.6
  156.0 2.3 collective-permute-done.3
  158.3 5.6 %collective-permute-start.4 = (bf16[516,256]{1,0:T(8,128)(2,1)S(1)}, bf16[516,256]{1,0:T(8,128)(2,1)S(1)}, u32[]{:S(2)}, u32[]{:S(2)}) collective-permute-start(bf16[516,256]{1,0:T(8,128)(2,1)S(1)} %collective-permute-done.3), channel_id=1, source_target_pairs={{0,1},{1,2},{2,3},{3,4},{4,5},{5,6},{6,7},{7,0},{8,9},{9,10},{10,1... | collective-permute-start | bytes 792584 | tf_op jit(solution)/shard_map/ppermute | solution.py:83
  164.0 2.1 collective-permute-start.7
  168.1 5.6 %collective-permute-done.7 = bf16[516,256]{1,0:T(8,128)(2,1)S(1)} collective-permute-done((bf16[516,256]{1,0:T(8,128)(2,1)S(1)}, bf16[516,256]{1,0:T(8,128)(2,1)S(1)}, u32[]{:S(2)}, u32[]{:S(2)}) %collective-permute-start.7) | collective-permute-done | bytes 264224 | tf_op jit(solution)/shard_map/ppermute | solution.py:85
  173.7 2.5 fusion.29
  177.8 7.1 %all-to-all-start.1 = ((bf16[8,516,256]{2,1,0:T(8,128)(2,1)}), bf16[8,516,256]{2,1,0:T(8,128)(2,1)S(1)}, u32[]{:S(2)}, u32[]{:S(2)}) async-start(bf16[8,516,256]{2,1,0:T(8,128)(2,1)} %broadcast_in_dim.5), calls=%async_computation.1 | async-start | bytes 4259840 | tf_op jit(solution)/shard_map/all_to_all | solution.py:32
  184.9 42.9 %all-to-all-done.1 = bf16[8,516,256]{2,1,0:T(8,128)(2,1)S(1)} async-done(((bf16[8,516,256]{2,1,0:T(8,128)(2,1)}), bf16[8,516,256]{2,1,0:T(8,128)(2,1)S(1)}, u32[]{:S(2)}, u32[]{:S(2)}) %all-to-all-start.1) | async-done | bytes 2113568 | tf_op jit(solution)/shard_map/all_to_all | solution.py:32
  234.1 7.4 %collective-permute-start.8 = (bf16[516,256]{1,0:T(8,128)(2,1)S(1)}, bf16[516,256]{1,0:T(8,128)(2,1)S(1)}, u32[]{:S(2)}, u32[]{:S(2)}) collective-permute-start(bf16[516,256]{1,0:T(8,128)(2,1)S(1)} %fusion.25), channel_id=1, source_target_pairs={{0,1},{1,2},{2,3},{3,4},{4,5},{5,6},{6,7},{7,0},{8,9},{9,10},{10,1... | collective-permute-start | bytes 792584 | tf_op jit(solution)/shard_map/ppermute | solution.py:83
  241.5 3.9 %collective-permute-done.8 = bf16[516,256]{1,0:T(8,128)(2,1)S(1)} collective-permute-done((bf16[516,256]{1,0:T(8,128)(2,1)S(1)}, bf16[516,256]{1,0:T(8,128)(2,1)S(1)}, u32[]{:S(2)}, u32[]{:S(2)}) %collective-permute-start.8) | collective-permute-done | bytes 264224 | tf_op jit(solution)/shard_map/ppermute | solution.py:83
  245.4 5.6 %collective-permute-start.9 = (bf16[516,256]{1,0:T(8,128)(2,1)S(1)}, bf16[516,256]{1,0:T(8,128)(2,1)S(1)}, u32[]{:S(2)}, u32[]{:S(2)}) collective-permute-start(bf16[516,256]{1,0:T(8,128)(2,1)S(1)} %collective-permute-done.8), channel_id=1, source_target_pairs={{0,1},{1,2},{2,3},{3,4},{4,5},{5,6},{6,7},{7,0},{8,9},{9,10},{10,1... | collective-permute-start | bytes 792584 | tf_op jit(solution)/shard_map/ppermute | solution.py:83
  251.0 2.0 collective-permute-start.12
  253.0 2.4 collective-permute-done.9
  255.4 5.6 %collective-permute-start.10 = (bf16[516,256]{1,0:T(8,128)(2,1)S(1)}, bf16[516,256]{1,0:T(8,128)(2,1)S(1)}, u32[]{:S(2)}, u32[]{:S(2)}) collective-permute-start(bf16[516,256]{1,0:T(8,128)(2,1)S(1)} %collective-permute-done.9), channel_id=1, source_target_pairs={{0,1},{1,2},{2,3},{3,4},{4,5},{5,6},{6,7},{7,0},{8,9},{9,10},{10,1... | collective-permute-start | bytes 792584 | tf_op jit(solution)/shard_map/ppermute | solution.py:83
  261.3 1.9 collective-permute-start.13
  263.3 3.3 %collective-permute-done.10 = bf16[516,256]{1,0:T(8,128)(2,1)S(1)} collective-permute-done((bf16[516,256]{1,0:T(8,128)(2,1)S(1)}, bf16[516,256]{1,0:T(8,128)(2,1)S(1)}, u32[]{:S(2)}, u32[]{:S(2)}) %collective-permute-start.10) | collective-permute-done | bytes 264224 | tf_op jit(solution)/shard_map/ppermute | solution.py:83
  266.6 5.6 %collective-permute-start.11 = (bf16[516,256]{1,0:T(8,128)(2,1)S(1)}, bf16[516,256]{1,0:T(8,128)(2,1)S(1)}, u32[]{:S(2)}, u32[]{:S(2)}) collective-permute-start(bf16[516,256]{1,0:T(8,128)(2,1)S(1)} %collective-permute-done.10), channel_id=1, source_target_pairs={{0,1},{1,2},{2,3},{3,4},{4,5},{5,6},{6,7},{7,0},{8,9},{9,10},{10,1... | collective-permute-start | bytes 792584 | tf_op jit(solution)/shard_map/ppermute | solution.py:83
  272.7 1.9 collective-permute-start.14
  276.4 5.9 %collective-permute-done.14 = bf16[516,256]{1,0:T(8,128)(2,1)S(1)} collective-permute-done((bf16[516,256]{1,0:T(8,128)(2,1)S(1)}, bf16[516,256]{1,0:T(8,128)(2,1)S(1)}, u32[]{:S(2)}, u32[]{:S(2)}) %collective-permute-start.14) | collective-permute-done | bytes 264224 | tf_op jit(solution)/shard_map/ppermute | solution.py:85
  (62 shorter events, 22.5 us)
Async XLA Ops:
  6.5 116.6 %all-gather.2.cloned.1.call-start = ((), (), s32[]{:S(2)}) async-start(), calls=%async_computation.2 | async-start | bytes 8650752 | tf_op jit(solution)/shard_map/all_gather | solution.py:21
  9.0 2.6 collective-permute-start
  14.2 42.7 %copy-start.1 = (bf16[2,2048]{1,0:T(2,128)(2,1)S(1)}, bf16[2,2048]{1,0:T(2,128)(2,1)}, u32[]{:S(2)}) copy-start(bf16[2,2048]{1,0:T(2,128)(2,1)} %param.10) | copy-start | bytes 24580
  14.2 42.7 %copy-start.2 = (bf16[2,3,256]{2,0,1:T(2,128)(2,1)S(1)}, bf16[2,3,256]{2,0,1:T(2,128)(2,1)}, u32[]{:S(2)}) copy-start(bf16[2,3,256]{2,0,1:T(2,128)(2,1)} %param.15) | copy-start | bytes 9220
  14.2 89.4 %all-to-all-start = ((bf16[8,516,256]{2,1,0:T(8,128)(2,1)}), bf16[8,516,256]{2,1,0:T(8,128)(2,1)S(1)}, u32[]{:S(2)}, u32[]{:S(2)}) async-start(bf16[8,516,256]{2,1,0:T(8,128)(2,1)} %broadcast_in_dim.4), calls=%async_computation | async-start | bytes 4259840 | tf_op jit(solution)/shard_map/all_to_all | solution.py:32
  129.2 10.4 %collective-permute-start.1 = (bf16[516,256]{1,0:T(8,128)(2,1)S(1)}, bf16[516,256]{1,0:T(8,128)(2,1)S(1)}, u32[]{:S(2)}, u32[]{:S(2)}) collective-permute-start(bf16[516,256]{1,0:T(8,128)(2,1)S(1)} %fusion.19), channel_id=1, source_target_pairs={{0,1},{1,2},{2,3},{3,4},{4,5},{5,6},{6,7},{7,0},{8,9},{9,10},{10,1... | collective-permute-start | bytes 792584 | tf_op jit(solution)/shard_map/ppermute | solution.py:83
  139.6 9.6 %collective-permute-start.2 = (bf16[516,256]{1,0:T(8,128)(2,1)S(1)}, bf16[516,256]{1,0:T(8,128)(2,1)S(1)}, u32[]{:S(2)}, u32[]{:S(2)}) collective-permute-start(bf16[516,256]{1,0:T(8,128)(2,1)S(1)} %collective-permute-done.1), channel_id=1, source_target_pairs={{0,1},{1,2},{2,3},{3,4},{4,5},{5,6},{6,7},{7,0},{8,9},{9,10},{10,1... | collective-permute-start | bytes 792584 | tf_op jit(solution)/shard_map/ppermute | solution.py:83
  143.2 10.8 %collective-permute-start.5 = (bf16[516,256]{1,0:T(8,128)(2,1)S(1)}, bf16[516,256]{1,0:T(8,128)(2,1)S(1)}, u32[]{:S(2)}, u32[]{:S(2)}) collective-permute-start(bf16[516,256]{1,0:T(8,128)(2,1)S(1)} %fusion.19), channel_id=1, source_target_pairs={{0,7},{1,0},{2,1},{3,2},{4,3},{5,4},{6,5},{7,6},{8,15},{9,8},{10,9... | collective-permute-start | bytes 792584 | tf_op jit(solution)/shard_map/ppermute | solution.py:85
  149.2 9.1 %collective-permute-start.3 = (bf16[516,256]{1,0:T(8,128)(2,1)S(1)}, bf16[516,256]{1,0:T(8,128)(2,1)S(1)}, u32[]{:S(2)}, u32[]{:S(2)}) collective-permute-start(bf16[516,256]{1,0:T(8,128)(2,1)S(1)} %collective-permute-done.2), channel_id=1, source_target_pairs={{0,1},{1,2},{2,3},{3,4},{4,5},{5,6},{6,7},{7,0},{8,9},{9,10},{10,1... | collective-permute-start | bytes 792584 | tf_op jit(solution)/shard_map/ppermute | solution.py:83
  154.0 10.0 %collective-permute-start.6 = (bf16[516,256]{1,0:T(8,128)(2,1)S(1)}, bf16[516,256]{1,0:T(8,128)(2,1)S(1)}, u32[]{:S(2)}, u32[]{:S(2)}) collective-permute-start(bf16[516,256]{1,0:T(8,128)(2,1)S(1)} %collective-permute-done.5), channel_id=1, source_target_pairs={{0,7},{1,0},{2,1},{3,2},{4,3},{5,4},{6,5},{7,6},{8,15},{9,8},{10,9... | collective-permute-start | bytes 792584 | tf_op jit(solution)/shard_map/ppermute | solution.py:85
  158.3 9.5 %collective-permute-start.4 = (bf16[516,256]{1,0:T(8,128)(2,1)S(1)}, bf16[516,256]{1,0:T(8,128)(2,1)S(1)}, u32[]{:S(2)}, u32[]{:S(2)}) collective-permute-start(bf16[516,256]{1,0:T(8,128)(2,1)S(1)} %collective-permute-done.3), channel_id=1, source_target_pairs={{0,1},{1,2},{2,3},{3,4},{4,5},{5,6},{6,7},{7,0},{8,9},{9,10},{10,1... | collective-permute-start | bytes 792584 | tf_op jit(solution)/shard_map/ppermute | solution.py:83
  163.9 9.7 %copy-start = (bf16[512,256]{1,0:T(8,128)(2,1)S(1)}, bf16[512,256]{1,0:T(8,128)(2,1)}, u32[]{:S(2)}) copy-start(bf16[512,256]{1,0:T(8,128)(2,1)} %param.9) | copy-start | bytes 786436
  164.0 9.7 %collective-permute-start.7 = (bf16[516,256]{1,0:T(8,128)(2,1)S(1)}, bf16[516,256]{1,0:T(8,128)(2,1)S(1)}, u32[]{:S(2)}, u32[]{:S(2)}) collective-permute-start(bf16[516,256]{1,0:T(8,128)(2,1)S(1)} %collective-permute-done.6), channel_id=1, source_target_pairs={{0,7},{1,0},{2,1},{3,2},{4,3},{5,4},{6,5},{7,6},{8,15},{9,8},{10,9... | collective-permute-start | bytes 792584 | tf_op jit(solution)/shard_map/ppermute | solution.py:85
  177.8 50.0 %all-to-all-start.1 = ((bf16[8,516,256]{2,1,0:T(8,128)(2,1)}), bf16[8,516,256]{2,1,0:T(8,128)(2,1)S(1)}, u32[]{:S(2)}, u32[]{:S(2)}) async-start(bf16[8,516,256]{2,1,0:T(8,128)(2,1)} %broadcast_in_dim.5), calls=%async_computation.1 | async-start | bytes 4259840 | tf_op jit(solution)/shard_map/all_to_all | solution.py:32
  228.3 2.2 slice-start
  228.8 3.0 %slice-start.1 = ((s8[8388608]{0:T(1024)(128)(4,1)}), s8[4194304]{0:T(1024)(128)(4,1)S(1)}, s32[]{:S(2)}) async-start(s8[8388608]{0:T(1024)(128)(4,1)} %bitcast.60), calls=%async_computation.4 | async-start | bytes 8388608
  234.1 11.3 %collective-permute-start.8 = (bf16[516,256]{1,0:T(8,128)(2,1)S(1)}, bf16[516,256]{1,0:T(8,128)(2,1)S(1)}, u32[]{:S(2)}, u32[]{:S(2)}) collective-permute-start(bf16[516,256]{1,0:T(8,128)(2,1)S(1)} %fusion.25), channel_id=1, source_target_pairs={{0,1},{1,2},{2,3},{3,4},{4,5},{5,6},{6,7},{7,0},{8,9},{9,10},{10,1... | collective-permute-start | bytes 792584 | tf_op jit(solution)/shard_map/ppermute | solution.py:83
  245.4 10.0 %collective-permute-start.9 = (bf16[516,256]{1,0:T(8,128)(2,1)S(1)}, bf16[516,256]{1,0:T(8,128)(2,1)S(1)}, u32[]{:S(2)}, u32[]{:S(2)}) collective-permute-start(bf16[516,256]{1,0:T(8,128)(2,1)S(1)} %collective-permute-done.8), channel_id=1, source_target_pairs={{0,1},{1,2},{2,3},{3,4},{4,5},{5,6},{6,7},{7,0},{8,9},{9,10},{10,1... | collective-permute-start | bytes 792584 | tf_op jit(solution)/shard_map/ppermute | solution.py:83
  251.0 10.3 %collective-permute-start.12 = (bf16[516,256]{1,0:T(8,128)(2,1)S(1)}, bf16[516,256]{1,0:T(8,128)(2,1)S(1)}, u32[]{:S(2)}, u32[]{:S(2)}) collective-permute-start(bf16[516,256]{1,0:T(8,128)(2,1)S(1)} %fusion.25), channel_id=1, source_target_pairs={{0,7},{1,0},{2,1},{3,2},{4,3},{5,4},{6,5},{7,6},{8,15},{9,8},{10,9... | collective-permute-start | bytes 792584 | tf_op jit(solution)/shard_map/ppermute | solution.py:85
  255.4 11.2 %collective-permute-start.10 = (bf16[516,256]{1,0:T(8,128)(2,1)S(1)}, bf16[516,256]{1,0:T(8,128)(2,1)S(1)}, u32[]{:S(2)}, u32[]{:S(2)}) collective-permute-start(bf16[516,256]{1,0:T(8,128)(2,1)S(1)} %collective-permute-done.9), channel_id=1, source_target_pairs={{0,1},{1,2},{2,3},{3,4},{4,5},{5,6},{6,7},{7,0},{8,9},{9,10},{10,1... | collective-permute-start | bytes 792584 | tf_op jit(solution)/shard_map/ppermute | solution.py:83
  261.3 11.4 %collective-permute-start.13 = (bf16[516,256]{1,0:T(8,128)(2,1)S(1)}, bf16[516,256]{1,0:T(8,128)(2,1)S(1)}, u32[]{:S(2)}, u32[]{:S(2)}) collective-permute-start(bf16[516,256]{1,0:T(8,128)(2,1)S(1)} %collective-permute-done.12), channel_id=1, source_target_pairs={{0,7},{1,0},{2,1},{3,2},{4,3},{5,4},{6,5},{7,6},{8,15},{9,8},{10,9... | collective-permute-start | bytes 792584 | tf_op jit(solution)/shard_map/ppermute | solution.py:85
  266.6 9.5 %collective-permute-start.11 = (bf16[516,256]{1,0:T(8,128)(2,1)S(1)}, bf16[516,256]{1,0:T(8,128)(2,1)S(1)}, u32[]{:S(2)}, u32[]{:S(2)}) collective-permute-start(bf16[516,256]{1,0:T(8,128)(2,1)S(1)} %collective-permute-done.10), channel_id=1, source_target_pairs={{0,1},{1,2},{2,3},{3,4},{4,5},{5,6},{6,7},{7,0},{8,9},{9,10},{10,1... | collective-permute-start | bytes 792584 | tf_op jit(solution)/shard_map/ppermute | solution.py:83
  272.7 9.5 %collective-permute-start.14 = (bf16[516,256]{1,0:T(8,128)(2,1)S(1)}, bf16[516,256]{1,0:T(8,128)(2,1)S(1)}, u32[]{:S(2)}, u32[]{:S(2)}) collective-permute-start(bf16[516,256]{1,0:T(8,128)(2,1)S(1)} %collective-permute-done.13), channel_id=1, source_target_pairs={{0,7},{1,0},{2,1},{3,2},{4,3},{5,4},{6,5},{7,6},{8,15},{9,8},{10,9... | collective-permute-start | bytes 792584 | tf_op jit(solution)/shard_map/ppermute | solution.py:85
Sparse Core Ops, SparseCore 0:
  9.5 113.5 all-gather.1
